TPU v7x, 32 devices: a whole 2x2x4 slice. The times are simulated.
32 devices in a mesh: ep: 8 (over z, x), tp: 4 (over y, core).
Axes of the slice: x: 2, y: 2, z: 4, core: 2. Of those that a mesh axis runs over, the one named last changes fastest.
Arguments:
- mix_input: bfloat16 [4096, 2048], P('ep', 'tp'), may hold values from -6 to 6
- mix_weight: bfloat16 [2048, 4096], P(None, 'tp'), may hold values from -0.125 to 0.125
- expert_input: bfloat16 [1024, 4096], P('ep', 'tp'), may hold values from -4500 to 4500
- expert_index: int32 [1024, 2], P('ep'), may hold values from 0 to 7, as said below
- route_share: float32 [1024, 2], P('ep'), may hold values from 0.1 to 1
- norm_gain: float32 [4096], replicated, may hold values from 0.1 to 1.9
- gate_weight: bfloat16 [8, 4096, 2048], P('ep', None, 'tp'), may hold values from -0.09375 to 0.09375
- up_weight: bfloat16 [8, 4096, 2048], P('ep', None, 'tp'), may hold values from -0.09375 to 0.09375
- down_weight: bfloat16 [8, 2048, 4096], P('ep', None, 'tp'), may hold values from -0.125 to 0.125
Outputs:
- mixed_rows: bfloat16 [4096, 4096], P('ep', 'tp')
- expert_rows: bfloat16 [1024, 4096], P('ep', 'tp')
Inputs may be any that keep to these rules, and one draw needn't show every extreme that they name: `expert_index`: each row names 2 different experts. Within each aligned block of 128 rows (the rows of one index of ep) no expert is named by more than 64 rows, and one expert, the same in every block, is named by exactly 64 rows.
All inputs are finite; a program needn't handle non-finite values.
Results may differ from a plain program's by a relative error of at most 0.007.
Values may be sent and summed in bfloat16 or wider, within the bound.
A program may use at most 64 MiB of HBM per device.

v0:
```python
import functools

import jax
import jax.numpy as jnp
from jax import lax
from jax.experimental import pallas as pl
from jax.experimental.pallas import tpu as pltpu
from jax.sharding import PartitionSpec as P

TOP = 2
HALO = 16
BATCHES = 4
POOL_AT = 3
GROUPS = 4
norm_eps = 1e-06
MESH = pl.DeviceIdType.MESH
F32 = jnp.float32
BF16 = jnp.bfloat16


def peer_order(n_ep):
    near = list(range(2, n_ep // 2))
    far = list(range(n_ep // 2, n_ep, 2)) + list(range(n_ep // 2 + 1, n_ep, 2))
    mixed = [x for pair in zip(far, near) for x in pair]
    return [0, 1] + mixed + far[len(near) :]


def dot(a, b):
    return jnp.dot(a, b, preferred_element_type=F32)


def kernel(
    n_ep, n_tp, cap,
    mix_ref, x_ref, idx_ref, share_ref, gain_ref, wm_hbm, wg_hbm, wu_hbm, wd_hbm,
    mixed_ref, rows_ref,
    wm, wg, wu, wd, out, tok, scaled, inv, hid, pool, prod, ret, halo, wcomb,
    w_sem, halo_sem, a2a_send, a2a_recv, back_send, back_recv,
    ty_send, ty_recv, tc_send, tc_recv,
    hy_send, hy_recv, hc_send, hc_recv,
    py_send, py_recv, pc_send, pc_recv,
):
    e = lax.axis_index("ep")
    t = lax.axis_index("tp")
    n_y = n_tp // 2
    pair = t + 1 - 2 * lax.rem(t, 2)
    tokens = x_ref.shape[0]
    fb = x_ref.shape[1]
    model = fb * n_tp
    length, channels = mix_ref.shape
    hb = wg.shape[1]
    ncols = wd.shape[1]
    gs = n_ep // BATCHES
    half = gs * cap
    order = peer_order(n_ep)

    def peer(i):
        return e ^ order[i]

    weights = [
        pltpu.make_async_copy(src, dst, w_sem.at[i])
        for i, (src, dst) in enumerate(
            ((wg_hbm.at[0], wg), (wu_hbm.at[0], wu), (wd_hbm.at[0], wd), (wm_hbm, wm))
        )
    ]
    for copy in weights:
        copy.start()

    barrier = pltpu.get_barrier_semaphore()
    for s in range(1, n_ep):
        pl.semaphore_signal(
            barrier, inc=1, device_id=(peer(s), t), device_id_type=MESH
        )
    for s in range(1, n_tp):
        pl.semaphore_signal(
            barrier, inc=1, device_id=(e, lax.rem(t + s, n_tp)), device_id_type=MESH
        )

    dest = jnp.concatenate(
        [jnp.full((1, tokens), peer(i), jnp.int32) for i in range(n_ep)], axis=0
    )
    first = idx_ref[0:1, :] == dest
    second = idx_ref[1:2, :] == dest
    named = jnp.where(first | second, 1.0, 0.0)
    total = share_ref[0:1, :] + share_ref[1:2, :]
    weight = jnp.where(first, share_ref[0:1, :] / total, 0.0) + jnp.where(
        second, share_ref[1:2, :] / total, 0.0
    )
    before = lax.broadcasted_iota(jnp.int32, (tokens, tokens), 0) < lax.broadcasted_iota(
        jnp.int32, (tokens, tokens), 1
    )
    slot = dot(named.astype(BF16), jnp.where(before, 1.0, 0.0).astype(BF16))
    slot = jnp.where(named > 0.0, slot, -1.0)
    slot_row = lax.broadcasted_iota(jnp.int32, (cap, tokens), 0).astype(F32)

    def chosen(s):
        return slot[s : s + 1, :] == slot_row

    def remote(src, dst, send, recv, dev):
        return pltpu.make_async_remote_copy(
            src_ref=src, dst_ref=dst, send_sem=send, recv_sem=recv,
            device_id=dev, device_id_type=MESH,
        )

    sends = []

    def go(*args):
        copy = remote(*args)
        copy.start()
        sends.append(copy)

    def gather_start(view, ys, yr, cs, cr):
        for d in range(1, n_y):
            go(view(t), view(t), ys.at[d], yr.at[d], (e, lax.rem(t + 2 * d, n_tp)))
        go(view(t), view(t), cs.at[0], cr.at[0], (e, pair))

    def gather_relay(view, ys, yr, cs, cr):
        for d in range(1, n_y):
            got = view(lax.rem(t + n_tp - 2 * d, n_tp))
            remote(got, got, ys.at[d], yr.at[d], (e, pair)).wait_recv()
            go(got, got, cs.at[d], cr.at[d], (e, pair))

    def gather_finish(view, ys, yr, cs, cr):
        for d in range(n_y):
            got = view(lax.rem(pair + n_tp - 2 * d, n_tp))
            remote(got, got, cs.at[d], cr.at[d], (e, pair)).wait_recv()

    def tok_args(s):
        return (lambda b: tok.at[b, s], ty_send.at[s], ty_recv.at[s], tc_send.at[s], tc_recv.at[s])

    def hid_args(h):
        return (
            lambda b: hid.at[b, pl.ds(h * half, half)],
            hy_send.at[h], hy_recv.at[h], hc_send.at[h], hc_recv.at[h],
        )

    pool_args = (lambda b: pool.at[b], py_send, py_recv, pc_send, pc_recv)

    tok[t, 0] = dot(jnp.where(chosen(0), 1.0, 0.0).astype(BF16), x_ref[...]).astype(BF16)
    pl.semaphore_wait(barrier, n_ep + n_tp - 2)

    go(mix_ref.at[pl.ds(length - HALO, HALO)], halo, halo_sem.at[0], halo_sem.at[1],
       (lax.rem(e + 1, n_ep), t))
    for s in range(1, n_ep):
        out[s] = dot(jnp.where(chosen(s), 1.0, 0.0).astype(BF16), x_ref[...]).astype(BF16)
        go(out.at[s], tok.at[t, s], a2a_send.at[s], a2a_recv.at[s], (peer(s), t))
        if s == 1:
            gather_start(*tok_args(0))

    spread = jnp.concatenate(
        [jnp.where(chosen(s), weight[s : s + 1, :], 0.0) for s in range(n_ep)], axis=0
    ).T
    high = spread.astype(BF16)
    wcomb[0] = high
    wcomb[1] = (spread - high.astype(F32)).astype(BF16)

    remote(halo, halo, halo_sem.at[0], halo_sem.at[1], (e, pair)).wait_recv()
    group = (t * channels) // (channels * n_tp // GROUPS)
    trailing = jnp.where(e == 0, 0.0, halo[...].astype(F32))
    own = mix_ref[...].astype(F32)
    running = jnp.concatenate([trailing, own], axis=0)
    running = running + pltpu.roll(running, 1, 0)
    for level in range(1, GROUPS):
        wider = running + pltpu.roll(running, 2**level, 0)
        running = jnp.where(group >= level, wider, running)
    window = jnp.int32(2)
    for level in range(1, GROUPS):
        window = jnp.where(group >= level, 2 ** (level + 1), window)
    position = e * length + lax.broadcasted_iota(jnp.int32, (length, 1), 0)
    counts = jnp.minimum(position + 1, window).astype(F32)
    pool[t] = (running[HALO:] / counts - own).astype(BF16)

    def hidden_half(h):
        for s in range(h * gs, (h + 1) * gs):
            gather_finish(*tok_args(s))

        @pl.loop(h * gs, (h + 1) * gs)
        def _(s):
            at = pl.ds(pl.multiple_of(s * cap, cap), cap)
            squares = jnp.zeros((cap, 1), F32)
            for b in range(n_tp):
                x = tok[b, s].astype(F32)
                squares = squares + jnp.sum(x * x, axis=1, keepdims=True)
                cols = slice(b * fb, (b + 1) * fb)
                scaled[at, cols] = (x * gain_ref[:, cols]).astype(BF16)
            inv[at, :] = lax.rsqrt(squares / model + norm_eps)

        if h == 0:
            weights[0].wait()
            weights[1].wait()
        at = pl.ds(h * half, half)
        wide = min(256, hb)

        @pl.loop(0, hb // wide)
        def _(n):
            cols = pl.ds(pl.multiple_of(n * wide, wide), wide)
            lhs = scaled[at, :]
            g = dot(lhs, wg[:, cols]) * inv[at, :]
            u = dot(lhs, wu[:, cols]) * inv[at, :]
            hid[t, at, cols] = (g / (1.0 + jnp.exp(-g)) * u).astype(BF16)

    def down_half(h):
        gather_finish(*hid_args(h))
        if h == 0:
            weights[2].wait()
        at = pl.ds(h * half, half)
        wide = min(256, ncols)

        @pl.loop(0, ncols // wide)
        def _(n):
            cols = pl.ds(pl.multiple_of(n * wide, wide), wide)
            acc = dot(hid[0, at, :], wd[0:hb, cols])
            for b in range(1, n_tp):
                acc = acc + dot(hid[b, at, :], wd[b * hb : (b + 1) * hb, cols])
            prod[at, cols] = acc.astype(BF16)

        for s in range(h * gs, (h + 1) * gs):
            rows = pl.ds(s * cap, cap)
            if s == 0:
                ret[rows, :] = prod[rows, :]
            else:
                go(prod.at[rows], ret.at[rows], back_send.at[s], back_recv.at[s], (peer(s), t))

    def stage(h):
        hidden_half(h)
        gather_start(*hid_args(h))
        if h == POOL_AT:
            gather_start(*pool_args)
        if h >= 1:
            gather_relay(*hid_args(h - 1))
            down_half(h - 1)

    lag = 2
    staged = 0
    for s in range(1, n_ep):
        got = tok.at[t, s]
        remote(got, got, a2a_send.at[s], a2a_recv.at[s], (e, pair)).wait_recv()
        gather_start(*tok_args(s))
        if s >= lag:
            gather_relay(*tok_args(s - lag))
        if s == (staged + 1) * gs + 3:
            stage(staged)
            staged += 1
    for s in range(n_ep - lag, n_ep):
        gather_relay(*tok_args(s))
    for h in range(staged, BATCHES):
        stage(h)
    gather_relay(*hid_args(BATCHES - 1))
    down_half(BATCHES - 1)

    gather_relay(*pool_args)
    gather_finish(*pool_args)
    weights[3].wait()
    wide = min(256, ncols)

    @pl.loop(0, ncols // wide)
    def _(n):
        cols = pl.ds(pl.multiple_of(n * wide, wide), wide)
        acc = dot(pool[0], wm[0:channels, cols])
        for b in range(1, n_tp):
            acc = acc + dot(pool[b], wm[b * channels : (b + 1) * channels, cols])
        mixed_ref[:, cols] = acc.astype(BF16)

    for s in range(1, n_ep):
        got = ret.at[pl.ds(s * cap, cap)]
        remote(got, got, back_send.at[s], back_recv.at[s], (e, pair)).wait_recv()

    @pl.loop(0, ncols // wide)
    def _(n):
        cols = pl.ds(pl.multiple_of(n * wide, wide), wide)
        back = ret[:, cols]
        rows_ref[:, cols] = (dot(wcomb[0], back) + dot(wcomb[1], back)).astype(BF16)

    for copy in sends:
        copy.wait_send()


def write_out(mixed_ref, rows_ref, mixed_out, rows_out):
    mixed_out[...] = mixed_ref[...]
    rows_out[...] = rows_ref[...]


def shards(
    n_ep, n_tp,
    mix_input, mix_weight, expert_input, expert_index, route_share, norm_gain,
    gate_weight, up_weight, down_weight,
):
    length, channels = mix_input.shape
    tokens, fb = expert_input.shape
    model = norm_gain.shape[0]
    hb = gate_weight.shape[2]
    ff = down_weight.shape[1]
    ncols = down_weight.shape[2]
    cap = 2 * tokens * TOP // n_ep
    slots = n_ep * cap
    n_y = n_tp // 2
    vmem = pl.BlockSpec(memory_space=pltpu.VMEM)
    anyspace = pl.BlockSpec(memory_space=pl.ANY)
    sem = pltpu.SemaphoreType.DMA
    mixed, rows = pl.pallas_call(
        functools.partial(kernel, n_ep, n_tp, cap),
        out_shape=(
            jax.ShapeDtypeStruct((length, ncols), BF16),
            jax.ShapeDtypeStruct((tokens, ncols), BF16),
        ),
        in_specs=[vmem] * 5 + [anyspace] * 4,
        out_specs=(vmem, vmem),
        scratch_shapes=[
            pltpu.VMEM(mix_weight.shape, BF16),
            pltpu.VMEM((model, hb), BF16),
            pltpu.VMEM((model, hb), BF16),
            pltpu.VMEM((ff, ncols), BF16),
            pltpu.VMEM((n_ep, cap, fb), BF16),
            pltpu.VMEM((n_tp, n_ep, cap, fb), BF16),
            pltpu.VMEM((slots, model), BF16),
            pltpu.VMEM((slots, 1), F32),
            pltpu.VMEM((n_tp, slots, hb), BF16),
            pltpu.VMEM((n_tp, length, channels), BF16),
            pltpu.VMEM((slots, ncols), BF16),
            pltpu.VMEM((slots, ncols), BF16),
            pltpu.VMEM((HALO, channels), BF16),
            pltpu.VMEM((2, tokens, slots), BF16),
            sem((4,)), sem((2,)),
            sem((n_ep,)), sem((n_ep,)), sem((n_ep,)), sem((n_ep,)),
            sem((n_ep, n_y)), sem((n_ep, n_y)), sem((n_ep, n_y)), sem((n_ep, n_y)),
            *[sem((BATCHES, n_y))] * 4,
            sem((n_y,)), sem((n_y,)), sem((n_y,)), sem((n_y,)),
        ],
        compiler_params=pltpu.CompilerParams(
            collective_id=0, has_side_effects=True, vmem_limit_bytes=60 * 1024 * 1024
        ),
    )(
        mix_input, expert_input, expert_index.T, route_share.T, norm_gain[None, :],
        mix_weight, gate_weight, up_weight, down_weight,
    )
    return pl.pallas_call(
        write_out,
        out_shape=(
            jax.ShapeDtypeStruct(mixed.shape, BF16),
            jax.ShapeDtypeStruct(rows.shape, BF16),
        ),
        in_specs=[vmem] * 2,
        out_specs=(vmem, vmem),
    )(mixed, rows)


def solution(mesh):
    placed = (
        P("ep", "tp"),
        P(None, "tp"),
        P("ep", "tp"),
        P("ep", None),
        P("ep", None),
        P(),
        P("ep", None, "tp"),
        P("ep", None, "tp"),
        P("ep", None, "tp"),
    )
    return jax.shard_map(
        functools.partial(shards, mesh.shape["ep"], mesh.shape["tp"]),
        mesh=mesh,
        in_specs=placed,
        out_specs=(P("ep", "tp"), P("ep", "tp")),
        check_vma=False,
    )
```

profile of v0, /device:TPU:0, one launch (start us, length us, event | category | flops | bytes accessed | tf_op | source)
XLA Modules:
  0.0 70.9 jit_solution(13878470722095043894)
XLA Ops:
  0.6 67.8 %shard_map.104 = (bf16[512,1024]{1,0:T(8,128)(2,1)}, bf16[128,1024]{1,0:T(8,128)(2,1)}) custom-call(bf16[512,512]{1,0:T(8,128)(2,1)} %mix_ref.1, bf16[128,1024]{1,0:T(8,128)(2,1)} %x_ref.1, s32[2,128]{1,0:T(2,128)} %bitcast.4, f32[2,128]{1,0:T(2,128)} %bitcast.5, f32[1,4096]{1,0:T(1,128)} %bitcast.3, bf16[2048,1024]{1,0:T(8,128)(2,1)} %wm_hbm.1, ...), custom_call_target="tpu_custom_call" | custom-call | tf_op jit(solution)/shard_map/pallas_call | solution.py:299
  68.5 2.4 %shard_map.105 = (bf16[512,1024]{1,0:T(8,128)(2,1)}, bf16[128,1024]{1,0:T(8,128)(2,1)}) custom-call(bf16[512,1024]{1,0:T(8,128)(2,1)} %get-tuple-element.4.mixed_ref, bf16[128,1024]{1,0:T(8,128)(2,1)} %get-tuple-element.5.rows_ref), custom_call_target="tpu_custom_call" | custom-call | tf_op jit(solution)/shard_map/pallas_call | solution.py:335
where the time goes:
time: 71 us; the launch traced here: 70.9 us
  Pallas kernels  70.2 us (99%)
    pallas_call x1, Pallas kernels, shards(): pl.pallas_call(functools.partial(kernel, n_ep, n_tp, cap), out_shape=(jax...  67.8 us
    pallas_call x1, Pallas kernels, shards(): pl.pallas_call(write_out, out_shape=(jax.ShapeDtypeStruct(mixed.shape, BF...  2.38 us

commit v1 on v0

v1 whole, which is shorter than its diff:
```python
import functools

import jax
import jax.numpy as jnp
from jax import lax
from jax.experimental import pallas as pl
from jax.experimental.pallas import tpu as pltpu
from jax.sharding import PartitionSpec as P

TOP = 2
HALO = 16
STAGES = 8
CHUNKS = 4
GROUPS = 4
norm_eps = 1e-06
LIMIT = 48 * 1024 * 1024
MESH = pl.DeviceIdType.MESH
F32 = jnp.float32
BF16 = jnp.bfloat16

PLAN = (
    ("send", 7), ("send", 5), ("barrier",), ("halo",), ("xown",), ("push", 7), ("send", 1),
    ("push", 5), ("send", 2), ("push", 1), ("push", 2), ("pool",), ("pstart", 0), ("xrel",),
    ("push2", 2), ("push2", 1), ("send", 6), ("send", 3), ("send", 4), ("pstart", 3),
    ("ownsel",), ("recv", 7), ("expert", 0, 1), ("push", 6), ("nrecv", 2), ("prelay", 0),
    ("prelay", 3), ("recv", 5), ("push", 3), ("relay", 7), ("expert", 2, 1), ("hrelay", 0, 1),
    ("push", 4), ("expert", 7, 1), ("push2", 3), ("relay", 5), ("recv", 6), ("expert", 5, 1),
    ("hrelay", 7, 1), ("nrecv", 1), ("hrelay", 2, 1), ("down", 7, 1), ("relay", 6), ("recv", 4),
    ("expert", 1, 1), ("hrelay", 5, 1), ("expert", 6, 1), ("nrecv", 3), ("down", 5, 1),
    ("pstart", 1), ("relay", 4), ("down", 2, 1), ("expert", 3, 1), ("hrelay", 6, 1),
    ("expert", 4, 1), ("down", 6, 1), ("hrelay", 4, 1), ("hrelay", 3, 1), ("pstart", 2),
    ("hrelay", 1, 1), ("down", 1, 1), ("down", 3, 1), ("down", 4, 1), ("prelay", 2),
    ("mixed", 3, 1), ("mixed", 0, 1), ("mixed", 2, 1), ("prelay", 1), ("down", 0, 1),
    ("mixed", 1, 1),
)


def dot(a, b):
    return jnp.dot(a, b, preferred_element_type=F32)


def kernel(
    n_ep, n_tp, cap,
    mix_hbm, x_hbm, idx_hbm, share_hbm, gain_hbm, wm_hbm, wg_hbm, wu_hbm, wd_hbm,
    mixed_ref, rows_ref,
    mix_ref, x_ref, idx_ref, share_ref, gain_ref, wm, wg, wu, wd, out, tok, scaled, inv, hid, pool, prod, ret, halo, wcomb, gathered,
    in_sem, w_sem, halo_sem, xy_send, xy_recv, xc_send, xc_recv, a2a_send, a2a_recv, back_send, back_recv,
    ty_send, ty_recv, tc_send, tc_recv,
    hy_send, hy_recv, hc_send, hc_recv,
    py_send, py_recv, pc_send, pc_recv,
):
    e = lax.axis_index("ep")
    t = lax.axis_index("tp")
    n_y = n_tp // 2
    pair = t + 1 - 2 * lax.rem(t, 2)
    tokens = x_ref.shape[0]
    fb = x_ref.shape[1]
    model = fb * n_tp
    length, channels = mix_ref.shape
    hb = wg.shape[1]
    ncols = wd.shape[1]
    gs = n_ep // STAGES
    half = gs * cap
    piece = length // CHUNKS

    def peer(s):
        return e ^ s

    def members(h):
        return range(h * gs, (h + 1) * gs)

    def others(h):
        return [s for s in members(h) if s]

    inputs = [
        pltpu.make_async_copy(src, dst, in_sem.at[i])
        for i, (src, dst) in enumerate(
            (
                (idx_hbm, idx_ref), (x_hbm, x_ref), (mix_hbm, mix_ref),
                (share_hbm, share_ref), (gain_hbm, gain_ref),
            )
        )
    ]
    for copy in inputs:
        copy.start()
    weights = [
        pltpu.make_async_copy(src, dst, w_sem.at[i])
        for i, (src, dst) in enumerate(
            ((wg_hbm.at[0], wg), (wu_hbm.at[0], wu), (wd_hbm.at[0], wd), (wm_hbm, wm))
        )
    ]
    loaded = set()

    def need(i):
        if i not in loaded:
            loaded.add(i)
            weights[i].wait()

    barrier = pltpu.get_barrier_semaphore()
    for s in range(1, n_ep):
        pl.semaphore_signal(
            barrier, inc=1, device_id=(peer(s), t), device_id_type=MESH
        )
    for s in range(1, n_tp):
        pl.semaphore_signal(
            barrier, inc=1, device_id=(e, lax.rem(t + s, n_tp)), device_id_type=MESH
        )
    for copy in weights:
        copy.start()
    inputs[0].wait()

    dest = jnp.concatenate(
        [jnp.full((1, tokens), peer(s), jnp.int32) for s in range(n_ep)], axis=0
    )
    first = idx_ref[0:1, :] == dest
    second = idx_ref[1:2, :] == dest
    named = jnp.where(first | second, 1.0, 0.0)
    before = lax.broadcasted_iota(jnp.int32, (tokens, tokens), 0) < lax.broadcasted_iota(
        jnp.int32, (tokens, tokens), 1
    )
    slot = dot(named.astype(BF16), jnp.where(before, 1.0, 0.0).astype(BF16))
    slot = jnp.where(named > 0.0, slot, -1.0)
    slot_row = lax.broadcasted_iota(jnp.int32, (cap, tokens), 0).astype(F32)

    def chosen(s):
        return slot[s : s + 1, :] == slot_row

    inputs[1].wait()

    def remote(src, dst, send, recv, dev):
        return pltpu.make_async_remote_copy(
            src_ref=src, dst_ref=dst, send_sem=send, recv_sem=recv,
            device_id=dev, device_id_type=MESH,
        )

    sends = []

    def go(*args):
        copy = remote(*args)
        copy.start()
        sends.append(copy)

    def gather_start(view, ys, yr, cs, cr):
        for d in range(1, n_y):
            go(view(t), view(t), ys.at[d], yr.at[d], (e, lax.rem(t + 2 * d, n_tp)))
        go(view(t), view(t), cs.at[0], cr.at[0], (e, pair))

    def gather_relay(view, ys, yr, cs, cr):
        for d in range(1, n_y):
            got = view(lax.rem(t + n_tp - 2 * d, n_tp))
            remote(got, got, ys.at[d], yr.at[d], (e, pair)).wait_recv()
            go(got, got, cs.at[d], cr.at[d], (e, pair))

    def gather_finish(view, ys, yr, cs, cr):
        for d in range(n_y):
            got = view(lax.rem(pair + n_tp - 2 * d, n_tp))
            remote(got, got, cs.at[d], cr.at[d], (e, pair)).wait_recv()

    def tok_args(s):
        return (lambda b: tok.at[b, s], ty_send.at[s], ty_recv.at[s], tc_send.at[s], tc_recv.at[s])

    def hid_args(h, n):
        return (
            lambda b: hid.at[b, pl.ds(h * half, n * half)],
            hy_send.at[h], hy_recv.at[h], hc_send.at[h], hc_recv.at[h],
        )

    def pool_args(c):
        return (
            lambda b: pool.at[b, pl.ds(c * piece, piece)],
            py_send.at[c], py_recv.at[c], pc_send.at[c], pc_recv.at[c],
        )

    def pick(s, x):
        return dot(jnp.where(chosen(s), 1.0, 0.0).astype(BF16), x).astype(BF16)

    def behind(d):
        return lax.rem(t + n_tp - 2 * d, n_tp)

    def near(s):
        return s < n_ep // 2

    def carry(s, d):
        b = behind(d)
        go(out.at[s, d], tok.at[b, s], a2a_send.at[s, d], a2a_recv.at[s, d], (peer(s), t))

    def send(h):
        for s in others(h):
            out[s, 0] = pick(s, x_ref[...])

    def push(h):
        for s in others(h):
            carry(s, 0)

    def xown():
        for d in range(1, n_y):
            go(x_ref, gathered.at[t], xy_send.at[d], xy_recv.at[d], (e, lax.rem(t + 2 * d, n_tp)))
        go(x_ref, gathered.at[t], xc_send.at[0], xc_recv.at[0], (e, pair))

    def xrel():
        gather_relay(lambda b: gathered.at[b], xy_send, xy_recv, xc_send, xc_recv)

    def push2(h):
        for d in range(1, n_y):
            x = gathered[behind(d)]
            for s in others(h):
                out[s, d] = pick(s, x)
                carry(s, d)

    def ownsel():
        gather_finish(lambda b: gathered.at[b], xy_send, xy_recv, xc_send, xc_recv)
        tok[t, 0] = pick(0, x_ref[...])
        for step in range(1, n_tp):
            b = lax.rem(t + step, n_tp)
            tok[b, 0] = pick(0, gathered[b])

    def nrecv(h):
        for s in others(h):
            for d in range(n_y):
                got = tok.at[behind(d), s]
                remote(got, got, a2a_send.at[s, d], a2a_recv.at[s, d], (e, pair)).wait_recv()
                go(got, got, tc_send.at[s, d], tc_recv.at[s, d], (e, pair))

    def halo_step():
        inputs[2].wait()
        go(mix_ref.at[pl.ds(length - HALO, HALO)], halo, halo_sem.at[0], halo_sem.at[1],
           (lax.rem(e + 1, n_ep), t))

    def pool_step():
        inputs[3].wait()
        inputs[4].wait()
        total = share_ref[0:1, :] + share_ref[1:2, :]
        weight = jnp.where(first, share_ref[0:1, :] / total, 0.0) + jnp.where(
            second, share_ref[1:2, :] / total, 0.0
        )
        spread = jnp.concatenate(
            [jnp.where(chosen(s), weight[s : s + 1, :], 0.0) for s in range(n_ep)], axis=0
        ).T
        high = spread.astype(BF16)
        wcomb[0] = high
        wcomb[1] = (spread - high.astype(F32)).astype(BF16)

        remote(halo, halo, halo_sem.at[0], halo_sem.at[1], (e, pair)).wait_recv()
        group = (t * channels) // (channels * n_tp // GROUPS)
        trailing = jnp.where(e == 0, 0.0, halo[...].astype(F32))
        own = mix_ref[...].astype(F32)
        running = jnp.concatenate([trailing, own], axis=0)
        running = running + pltpu.roll(running, 1, 0)
        for level in range(1, GROUPS):
            wider = running + pltpu.roll(running, 2**level, 0)
            running = jnp.where(group >= level, wider, running)
        window = jnp.int32(2)
        for level in range(1, GROUPS):
            window = jnp.where(group >= level, 2 ** (level + 1), window)
        position = e * length + lax.broadcasted_iota(jnp.int32, (length, 1), 0)
        counts = jnp.minimum(position + 1, window).astype(F32)
        pool[t] = (running[HALO:] / counts - own).astype(BF16)

    def recv(h):
        for s in others(h):
            got = tok.at[t, s]
            remote(got, got, a2a_send.at[s, 0], a2a_recv.at[s, 0], (e, pair)).wait_recv()
            gather_start(*tok_args(s))

    def relay(h):
        for s in members(h):
            gather_relay(*tok_args(s))

    def expert(h, n):
        for s in range(max(h * gs, 1), (h + n) * gs):
            gather_finish(*tok_args(s))

        @pl.loop(h * gs, (h + n) * gs)
        def _(s):
            at = pl.ds(pl.multiple_of(s * cap, cap), cap)
            squares = jnp.zeros((cap, 1), F32)
            for b in range(n_tp):
                x = tok[b, s].astype(F32)
                squares = squares + jnp.sum(x * x, axis=1, keepdims=True)
                cols = slice(b * fb, (b + 1) * fb)
                scaled[at, cols] = (x * gain_ref[:, cols]).astype(BF16)
            inv[at, :] = lax.rsqrt(squares / model + norm_eps)

        need(0)
        need(1)
        at = pl.ds(h * half, n * half)
        wide = min(512, hb)

        @pl.loop(0, hb // wide)
        def _(n):
            cols = pl.ds(pl.multiple_of(n * wide, wide), wide)
            lhs = scaled[at, :]
            g = dot(lhs, wg[:, cols]) * inv[at, :]
            u = dot(lhs, wu[:, cols]) * inv[at, :]
            hid[t, at, cols] = (g / (1.0 + jnp.exp(-g)) * u).astype(BF16)

        gather_start(*hid_args(h, n))

    def down(h, n):
        gather_finish(*hid_args(h, n))
        need(2)
        at = pl.ds(h * half, n * half)
        wide = min(512, ncols)

        @pl.loop(0, ncols // wide)
        def _(n):
            cols = pl.ds(pl.multiple_of(n * wide, wide), wide)
            acc = dot(hid[0, at, :], wd[0:hb, cols])
            for b in range(1, n_tp):
                acc = acc + dot(hid[b, at, :], wd[b * hb : (b + 1) * hb, cols])
            prod[at, cols] = acc.astype(BF16)

        for s in range(h * gs, (h + n) * gs):
            rows = pl.ds(s * cap, cap)
            if s == 0:
                ret[rows, :] = prod[rows, :]
            else:
                go(prod.at[rows], ret.at[rows], back_send.at[s], back_recv.at[s], (peer(s), t))

    def mixed_step(c, n):
        for i in range(c, c + n):
            gather_finish(*pool_args(i))
        need(3)
        at = pl.ds(c * piece, n * piece)
        wide = min(512, ncols)

        @pl.loop(0, ncols // wide)
        def _(n):
            cols = pl.ds(pl.multiple_of(n * wide, wide), wide)
            acc = dot(pool[0, at, :], wm[0:channels, cols])
            for b in range(1, n_tp):
                acc = acc + dot(pool[b, at, :], wm[b * channels : (b + 1) * channels, cols])
            mixed_ref[at, cols] = acc.astype(BF16)

    steps = {
        "send": send, "push": push, "xown": xown, "xrel": xrel, "push2": push2, "ownsel": ownsel, "nrecv": nrecv,
        "halo": halo_step, "pool": pool_step,
        "barrier": lambda: pl.semaphore_wait(barrier, n_ep + n_tp - 2),
        "recv": recv, "relay": relay, "expert": expert, "down": down,
        "hrelay": lambda h, n: gather_relay(*hid_args(h, n)),
        "pstart": lambda c: gather_start(*pool_args(c)),
        "prelay": lambda c: gather_relay(*pool_args(c)),
        "mixed": mixed_step,
    }
    for name, *arg in PLAN:
        steps[name](*arg)

    for s in range(1, n_ep):
        got = ret.at[pl.ds(s * cap, cap)]
        remote(got, got, back_send.at[s], back_recv.at[s], (e, pair)).wait_recv()
    wide = min(512, ncols)

    @pl.loop(0, ncols // wide)
    def _(n):
        cols = pl.ds(pl.multiple_of(n * wide, wide), wide)
        back = ret[:, cols]
        rows_ref[:, cols] = (dot(wcomb[0], back) + dot(wcomb[1], back)).astype(BF16)

    for copy in sends:
        copy.wait_send()


def write_out(mixed_ref, rows_ref, mixed_out, rows_out, done):
    copies = [
        pltpu.make_async_copy(mixed_ref, mixed_out, done.at[0]),
        pltpu.make_async_copy(rows_ref, rows_out, done.at[1]),
    ]
    for copy in copies:
        copy.start()
    for copy in copies:
        copy.wait()


def shards(
    n_ep, n_tp,
    mix_input, mix_weight, expert_input, expert_index, route_share, norm_gain,
    gate_weight, up_weight, down_weight,
):
    length, channels = mix_input.shape
    tokens, fb = expert_input.shape
    model = norm_gain.shape[0]
    hb = gate_weight.shape[2]
    ff = down_weight.shape[1]
    ncols = down_weight.shape[2]
    cap = 2 * tokens * TOP // n_ep
    slots = n_ep * cap
    n_y = n_tp // 2
    vmem = pl.BlockSpec(memory_space=pltpu.VMEM)
    hbm = pl.BlockSpec(memory_space=pltpu.HBM)
    sem = pltpu.SemaphoreType.DMA
    mixed, rows = pl.pallas_call(
        functools.partial(kernel, n_ep, n_tp, cap),
        out_shape=(
            pltpu.VMEM((length, ncols), BF16),
            pltpu.VMEM((tokens, ncols), BF16),
        ),
        in_specs=[hbm] * 9,
        out_specs=(vmem, vmem),
        scratch_shapes=[
            pltpu.VMEM(mix_input.shape, BF16),
            pltpu.VMEM(expert_input.shape, BF16),
            pltpu.VMEM((TOP, tokens), jnp.int32),
            pltpu.VMEM((TOP, tokens), F32),
            pltpu.VMEM((1, model), F32),
            pltpu.VMEM(mix_weight.shape, BF16),
            pltpu.VMEM((model, hb), BF16),
            pltpu.VMEM((model, hb), BF16),
            pltpu.VMEM((ff, ncols), BF16),
            pltpu.VMEM((n_ep, n_y, cap, fb), BF16),
            pltpu.VMEM((n_tp, n_ep, cap, fb), BF16),
            pltpu.VMEM((slots, model), BF16),
            pltpu.VMEM((slots, 1), F32),
            pltpu.VMEM((n_tp, slots, hb), BF16),
            pltpu.VMEM((n_tp, length, channels), BF16),
            pltpu.VMEM((slots, ncols), BF16),
            pltpu.VMEM((slots, ncols), BF16),
            pltpu.VMEM((HALO, channels), BF16),
            pltpu.VMEM((2, tokens, slots), BF16),
            pltpu.VMEM((n_tp, tokens, fb), BF16),
            sem((5,)), sem((4,)), sem((2,)), *[sem((n_y,))] * 4,
            sem((n_ep, n_y)), sem((n_ep, n_y)), sem((n_ep,)), sem((n_ep,)),
            sem((n_ep, n_y)), sem((n_ep, n_y)), sem((n_ep, n_y)), sem((n_ep, n_y)),
            *[sem((STAGES, n_y))] * 4,
            *[sem((CHUNKS, n_y))] * 4,
        ],
        compiler_params=pltpu.CompilerParams(
            collective_id=0, has_side_effects=True, vmem_limit_bytes=LIMIT
        ),
    )(
        *[
            pltpu.with_memory_space_constraint(x, pltpu.HBM)
            for x in (
                mix_input, expert_input, expert_index.T, route_share.T, norm_gain[None, :],
                mix_weight, gate_weight, up_weight, down_weight,
            )
        ]
    )
    return pl.pallas_call(
        write_out,
        out_shape=(
            jax.ShapeDtypeStruct(mixed.shape, BF16),
            jax.ShapeDtypeStruct(rows.shape, BF16),
        ),
        in_specs=[vmem] * 2,
        out_specs=(hbm, hbm),
        scratch_shapes=[sem((2,))],
    )(
        pltpu.with_memory_space_constraint(mixed, pltpu.VMEM),
        pltpu.with_memory_space_constraint(rows, pltpu.VMEM),
    )


def solution(mesh):
    placed = (
        P("ep", "tp"),
        P(None, "tp"),
        P("ep", "tp"),
        P("ep", None),
        P("ep", None),
        P(),
        P("ep", None, "tp"),
        P("ep", None, "tp"),
        P("ep", None, "tp"),
    )
    return jax.shard_map(
        functools.partial(shards, mesh.shape["ep"], mesh.shape["tp"]),
        mesh=mesh,
        in_specs=placed,
        out_specs=(P("ep", "tp"), P("ep", "tp")),
        check_vma=False,
    )
```

time: 71 us -> 62.5 us (0.88)
  Pallas kernels: 70.2 us -> 60.9 us
    pallas_call x1, Pallas kernels: 67.8 us -> 59.9 us  [shards(): pl.pallas_call(functools.partial(kernel, n_ep, n_tp, cap), out_shape=(plt...]
    pallas_call x1, Pallas kernels: 2.38 us -> 1.07 us  [shards(): pl.pallas_call(write_out, out_shape=(jax.ShapeDtypeStruct(mixed.shape, BF...]
where the time goes in v1:
time: 62.5 us; the launch traced here: 61.7 us
  Pallas kernels  60.9 us (97%)
  between operations  0.8 us (1%)
    pallas_call x1, Pallas kernels, shards(): pl.pallas_call(functools.partial(kernel, n_ep, n_tp, cap), out_shape=(plt...  59.9 us

profile of v1, /device:TPU:0, one launch (start us, length us, event | category | flops | bytes accessed | tf_op | source)
XLA Modules:
  0.0 61.7 jit_solution(1537436035162861453)
XLA Ops:
  0.6 59.9 %shard_map.104 = (bf16[512,1024]{1,0:T(8,128)(2,1)S(1)}, bf16[128,1024]{1,0:T(8,128)(2,1)S(1)}) custom-call(bf16[512,512]{1,0:T(8,128)(2,1)} %mix_hbm.1, bf16[128,1024]{1,0:T(8,128)(2,1)} %x_hbm.1, s32[2,128]{1,0:T(2,128)} %bitcast.4, f32[2,128]{1,0:T(2,128)} %bitcast.5, f32[1,4096]{1,0:T(1,128)} %bitcast.3, bf16[2048,1024]{1,0:T(8,128)(2,1)} %wm_hbm.1, ...), custom_call_target="tpu_custom_call" | custom-call | tf_op jit(solution)/shard_map/pallas_call | solution.py:391
  60.5 1.1 %shard_map.105 = (bf16[512,1024]{1,0:T(8,128)(2,1)}, bf16[128,1024]{1,0:T(8,128)(2,1)}) custom-call(bf16[512,1024]{1,0:T(8,128)(2,1)S(1)} %get-tuple-element.4.mixed_ref, bf16[128,1024]{1,0:T(8,128)(2,1)S(1)} %get-tuple-element.5.rows_ref), custom_call_target="tpu_custom_call" | custom-call | tf_op jit(solution)/shard_map/pallas_call | solution.py:438

commit v2 on v1

--- a/solution.py
+++ b/solution.py
@@ -19,19 +19,23 @@
 BF16 = jnp.bfloat16
 
 PLAN = (
-    ("send", 7), ("send", 5), ("barrier",), ("halo",), ("xown",), ("push", 7), ("send", 1),
-    ("push", 5), ("send", 2), ("push", 1), ("push", 2), ("pool",), ("pstart", 0), ("xrel",),
-    ("push2", 2), ("push2", 1), ("send", 6), ("send", 3), ("send", 4), ("pstart", 3),
-    ("ownsel",), ("recv", 7), ("expert", 0, 1), ("push", 6), ("nrecv", 2), ("prelay", 0),
-    ("prelay", 3), ("recv", 5), ("push", 3), ("relay", 7), ("expert", 2, 1), ("hrelay", 0, 1),
-    ("push", 4), ("expert", 7, 1), ("push2", 3), ("relay", 5), ("recv", 6), ("expert", 5, 1),
-    ("hrelay", 7, 1), ("nrecv", 1), ("hrelay", 2, 1), ("down", 7, 1), ("relay", 6), ("recv", 4),
-    ("expert", 1, 1), ("hrelay", 5, 1), ("expert", 6, 1), ("nrecv", 3), ("down", 5, 1),
-    ("pstart", 1), ("relay", 4), ("down", 2, 1), ("expert", 3, 1), ("hrelay", 6, 1),
-    ("expert", 4, 1), ("down", 6, 1), ("hrelay", 4, 1), ("hrelay", 3, 1), ("pstart", 2),
-    ("hrelay", 1, 1), ("down", 1, 1), ("down", 3, 1), ("down", 4, 1), ("prelay", 2),
-    ("mixed", 3, 1), ("mixed", 0, 1), ("mixed", 2, 1), ("prelay", 1), ("down", 0, 1),
-    ("mixed", 1, 1),
+    ("send", 7), ("barrier",), ("halo",), ("send", 0), ("push", 0), ("push", 7), ("send", 5),
+    ("push", 5), ("send", 2), ("push", 2), ("xown",), ("send", 1), ("pool",), ("pstart", 1),
+    ("xrel",), ("push2", 0), ("send", 6), ("send", 3), ("push2", 2), ("send", 4), ("recv", 7),
+    ("push", 1), ("push2", 1), ("pstart", 3), ("prelay", 1), ("push", 6), ("relay", 7),
+    ("recv", 5), ("nrecv", 2), ("ownsel",), ("nrecv", 0), ("scale", 7, 1), ("push", 3),
+    ("gu", 7, 1), ("scale", 2, 1), ("push", 4), ("expert", 7, 1), ("gu", 2, 1), ("expert", 2, 1),
+    ("relay", 5), ("recv", 6), ("push2", 3), ("scale", 5, 1), ("hrelay", 7, 1), ("nrecv", 1),
+    ("prelay", 3), ("gu", 5, 1), ("expert", 5, 1), ("hrelay", 2, 1), ("down", 7, 1),
+    ("scale", 1, 1), ("recv", 4), ("gu", 1, 1), ("relay", 6), ("expert", 1, 1), ("scale", 6, 1),
+    ("hrelay", 5, 1), ("gu", 6, 1), ("nrecv", 3), ("expert", 6, 1), ("pstart", 0),
+    ("down", 5, 1), ("scale", 3, 1), ("down", 2, 1), ("relay", 4), ("gu", 3, 1),
+    ("hrelay", 6, 1), ("expert", 3, 1), ("hrelay", 1, 1), ("scale", 4, 1), ("gu", 4, 1),
+    ("expert", 4, 1), ("down", 6, 1), ("scale", 0, 1), ("pstart", 2), ("hrelay", 3, 1),
+    ("gu", 0, 1), ("down", 1, 1), ("mixed", 3, 1), ("prelay", 0), ("down", 3, 1),
+    ("hrelay", 4, 1), ("down", 4, 1), ("expert", 0, 1), ("comb", 7, 1), ("mixed", 0, 1),
+    ("prelay", 2), ("comb", 5, 1), ("hrelay", 0, 1), ("comb", 6, 1), ("mixed", 1, 1),
+    ("mixed", 2, 1), ("down", 0, 1), ("comb", 0, 4), ("comb", 4, 1),
 )
 
 
@@ -43,7 +47,7 @@
     n_ep, n_tp, cap,
     mix_hbm, x_hbm, idx_hbm, share_hbm, gain_hbm, wm_hbm, wg_hbm, wu_hbm, wd_hbm,
     mixed_ref, rows_ref,
-    mix_ref, x_ref, idx_ref, share_ref, gain_ref, wm, wg, wu, wd, out, tok, scaled, inv, hid, pool, prod, ret, halo, wcomb, gathered,
+    mix_ref, x_ref, idx_ref, share_ref, gain_ref, wm, wg, wu, wd, out, tok, scaled, inv, hid, pool, prod, ret, halo, wcomb, gathered, total,
     in_sem, w_sem, halo_sem, xy_send, xy_recv, xc_send, xc_recv, a2a_send, a2a_recv, back_send, back_recv,
     ty_send, ty_recv, tc_send, tc_recv,
     hy_send, hy_recv, hc_send, hc_recv,
@@ -81,8 +85,6 @@
             )
         )
     ]
-    for copy in inputs:
-        copy.start()
     weights = [
         pltpu.make_async_copy(src, dst, w_sem.at[i])
         for i, (src, dst) in enumerate(
@@ -105,7 +107,7 @@
         pl.semaphore_signal(
             barrier, inc=1, device_id=(e, lax.rem(t + s, n_tp)), device_id_type=MESH
         )
-    for copy in weights:
+    for copy in inputs + weights:
         copy.start()
     inputs[0].wait()
 
@@ -233,12 +235,13 @@
         weight = jnp.where(first, share_ref[0:1, :] / total, 0.0) + jnp.where(
             second, share_ref[1:2, :] / total, 0.0
         )
-        spread = jnp.concatenate(
-            [jnp.where(chosen(s), weight[s : s + 1, :], 0.0) for s in range(n_ep)], axis=0
-        ).T
-        high = spread.astype(BF16)
-        wcomb[0] = high
-        wcomb[1] = (spread - high.astype(F32)).astype(BF16)
+        for h in range(STAGES):
+            spread = jnp.concatenate(
+                [jnp.where(chosen(s), weight[s : s + 1, :], 0.0) for s in members(h)], axis=0
+            ).T
+            high = spread.astype(BF16)
+            wcomb[0, h] = high
+            wcomb[1, h] = (spread - high.astype(F32)).astype(BF16)
 
         remote(halo, halo, halo_sem.at[0], halo_sem.at[1], (e, pair)).wait_recv()
         group = (t * channels) // (channels * n_tp // GROUPS)
@@ -266,7 +269,7 @@
         for s in members(h):
             gather_relay(*tok_args(s))
 
-    def expert(h, n):
+    def scale(h, n):
         for s in range(max(h * gs, 1), (h + n) * gs):
             gather_finish(*tok_args(s))
 
@@ -281,19 +284,26 @@
                 scaled[at, cols] = (x * gain_ref[:, cols]).astype(BF16)
             inv[at, :] = lax.rsqrt(squares / model + norm_eps)
 
+    def tall(x):
+        return jnp.concatenate([x, x], axis=0) if x.shape[0] <= 64 else x
+
+    def hidden(h, n, cols):
         need(0)
         need(1)
         at = pl.ds(h * half, n * half)
-        wide = min(512, hb)
-
-        @pl.loop(0, hb // wide)
-        def _(n):
-            cols = pl.ds(pl.multiple_of(n * wide, wide), wide)
-            lhs = scaled[at, :]
-            g = dot(lhs, wg[:, cols]) * inv[at, :]
-            u = dot(lhs, wu[:, cols]) * inv[at, :]
-            hid[t, at, cols] = (g / (1.0 + jnp.exp(-g)) * u).astype(BF16)
-
+        lhs = tall(scaled[at, :])
+        g = dot(lhs, wg[:, cols])[: n * half] * inv[at, :]
+        u = dot(lhs, wu[:, cols])[: n * half] * inv[at, :]
+        hid[t, at, cols] = (g / (1.0 + jnp.exp(-g)) * u).astype(BF16)
+
+    cut = hb // 2 if hb % 256 == 0 else 0
+
+    def gu(h, n):
+        if cut:
+            hidden(h, n, slice(0, cut))
+
+    def expert(h, n):
+        hidden(h, n, slice(cut, hb))
         gather_start(*hid_args(h, n))
 
     def down(h, n):
@@ -301,14 +311,10 @@
         need(2)
         at = pl.ds(h * half, n * half)
         wide = min(512, ncols)
-
-        @pl.loop(0, ncols // wide)
-        def _(n):
-            cols = pl.ds(pl.multiple_of(n * wide, wide), wide)
-            acc = dot(hid[0, at, :], wd[0:hb, cols])
-            for b in range(1, n_tp):
-                acc = acc + dot(hid[b, at, :], wd[b * hb : (b + 1) * hb, cols])
-            prod[at, cols] = acc.astype(BF16)
+        lhs = tall(jnp.concatenate([hid[b, at, :] for b in range(n_tp)], axis=1))
+        for n0 in range(0, ncols, wide):
+            cols = slice(n0, n0 + wide)
+            prod[at, cols] = dot(lhs, wd[:, cols])[: n * half].astype(BF16)
 
         for s in range(h * gs, (h + n) * gs):
             rows = pl.ds(s * cap, cap)
@@ -316,6 +322,26 @@
                 ret[rows, :] = prod[rows, :]
             else:
                 go(prod.at[rows], ret.at[rows], back_send.at[s], back_recv.at[s], (peer(s), t))
+
+    combs = [step for step in PLAN if step[0] == "comb"]
+
+    def comb(h, n):
+        for s in range(max(h * gs, 1), (h + n) * gs):
+            got = ret.at[pl.ds(s * cap, cap)]
+            remote(got, got, back_send.at[s], back_recv.at[s], (e, pair)).wait_recv()
+        wide = min(512, ncols)
+        for n0 in range(0, ncols, wide):
+            cols = slice(n0, n0 + wide)
+            acc = None if ("comb", h, n) == combs[0] else total[:, cols]
+            for i in range(h, h + n):
+                back = ret[pl.ds(i * half, half), cols]
+                for part in range(2):
+                    term = dot(wcomb[part, i], back)
+                    acc = term if acc is None else acc + term
+            if ("comb", h, n) == combs[-1]:
+                rows_ref[:, cols] = acc.astype(BF16)
+            else:
+                total[:, cols] = acc
 
     def mixed_step(c, n):
         for i in range(c, c + n):
@@ -336,7 +362,8 @@
         "send": send, "push": push, "xown": xown, "xrel": xrel, "push2": push2, "ownsel": ownsel, "nrecv": nrecv,
         "halo": halo_step, "pool": pool_step,
         "barrier": lambda: pl.semaphore_wait(barrier, n_ep + n_tp - 2),
-        "recv": recv, "relay": relay, "expert": expert, "down": down,
+        "recv": recv, "relay": relay, "scale": scale, "gu": gu, "expert": expert, "down": down,
+        "comb": comb,
         "hrelay": lambda h, n: gather_relay(*hid_args(h, n)),
         "pstart": lambda c: gather_start(*pool_args(c)),
         "prelay": lambda c: gather_relay(*pool_args(c)),
@@ -344,17 +371,6 @@
     }
     for name, *arg in PLAN:
         steps[name](*arg)
-
-    for s in range(1, n_ep):
-        got = ret.at[pl.ds(s * cap, cap)]
-        remote(got, got, back_send.at[s], back_recv.at[s], (e, pair)).wait_recv()
-    wide = min(512, ncols)
-
-    @pl.loop(0, ncols // wide)
-    def _(n):
-        cols = pl.ds(pl.multiple_of(n * wide, wide), wide)
-        back = ret[:, cols]
-        rows_ref[:, cols] = (dot(wcomb[0], back) + dot(wcomb[1], back)).astype(BF16)
 
     for copy in sends:
         copy.wait_send()
@@ -415,8 +431,9 @@
             pltpu.VMEM((slots, ncols), BF16),
             pltpu.VMEM((slots, ncols), BF16),
             pltpu.VMEM((HALO, channels), BF16),
-            pltpu.VMEM((2, tokens, slots), BF16),
+            pltpu.VMEM((2, STAGES, tokens, slots // STAGES), BF16),
             pltpu.VMEM((n_tp, tokens, fb), BF16),
+            pltpu.VMEM((tokens, ncols), F32),
             sem((5,)), sem((4,)), sem((2,)), *[sem((n_y,))] * 4,
             sem((n_ep, n_y)), sem((n_ep, n_y)), sem((n_ep,)), sem((n_ep,)),
             sem((n_ep, n_y)), sem((n_ep, n_y)), sem((n_ep, n_y)), sem((n_ep, n_y)),

time: 62.5 us -> 61.5 us (0.984); the launches traced: 61.7 us -> 61.4 us
  no operation moved by 1% of the time
where the time goes in v2:
time: 61.5 us; the launch traced here: 61.4 us
  Pallas kernels  60.6 us (99%)
  between operations  0.8 us (1%)
    pallas_call x1, Pallas kernels, shards(): pl.pallas_call(functools.partial(kernel, n_ep, n_tp, cap), out_shape=(plt...  59.5 us

profile of v2, /device:TPU:0, one launch (start us, length us, event | category | flops | bytes accessed | tf_op | source)
XLA Modules:
  0.0 61.4 jit_solution(6681540919856523368)
XLA Ops:
  0.6 59.5 %shard_map.104 = (bf16[512,1024]{1,0:T(8,128)(2,1)S(1)}, bf16[128,1024]{1,0:T(8,128)(2,1)S(1)}) custom-call(bf16[512,512]{1,0:T(8,128)(2,1)} %mix_hbm.1, bf16[128,1024]{1,0:T(8,128)(2,1)} %x_hbm.1, s32[2,128]{1,0:T(2,128)} %bitcast.4, f32[2,128]{1,0:T(2,128)} %bitcast.5, f32[1,4096]{1,0:T(1,128)} %bitcast.3, bf16[2048,1024]{1,0:T(8,128)(2,1)} %wm_hbm.1, ...), custom_call_target="tpu_custom_call" | custom-call | tf_op jit(solution)/shard_map/pallas_call | solution.py:407
  60.2 1.1 %shard_map.105 = (bf16[512,1024]{1,0:T(8,128)(2,1)}, bf16[128,1024]{1,0:T(8,128)(2,1)}) custom-call(bf16[512,1024]{1,0:T(8,128)(2,1)S(1)} %get-tuple-element.4.mixed_ref, bf16[128,1024]{1,0:T(8,128)(2,1)S(1)} %get-tuple-element.5.rows_ref), custom_call_target="tpu_custom_call" | custom-call | tf_op jit(solution)/shard_map/pallas_call | solution.py:455
